TPU v7x, 32 devices: a whole 2x2x4 slice. The times are simulated.
32 devices in a mesh: rep: 2 (over x), fs: 4 (over z), tp: 4 (over y, core).
Axes of the slice: x: 2, y: 2, z: 4, core: 2. Of those that a mesh axis runs over, the one named last changes fastest.
Arguments:
- tokens: bfloat16 [4096, 2048], P(('rep', 'fs', 'tp')), may hold values from -6 to 6
- mixer_gain: float32 [2048], replicated, may hold values from 0.1 to 1.9
- direct_weight: float32 [2048, 1024], P('fs', 'tp'), may hold values from -0.125 to 0.125
- direct_scale: float32 [1024], P('tp'), may hold values from 0.5 to 2
- value_weight: float32 [2048, 1024], P('fs', 'tp'), may hold values from -0.125 to 0.125
- value_scale: float32 [1024], P('tp'), may hold values from 0.5 to 8, as said below
- value_gain: float32 [1024], P('tp'), may hold values from 0.1 to 1.9
- value_shift: float32 [1024], P('tp'), may hold values from -3 to 3
- spatial_weight: bfloat16 [16, 128, 128], P('tp'), may hold values from -0.25 to 0.25
- spatial_bias: float32 [16, 128], P('tp'), may hold values from 0.1 to 1.9
- merge_weight: float32 [1024, 2048], P('tp', 'fs'), may hold values from -0.1875 to 0.1875
- merge_scale: float32 [2048], P('fs'), may hold values from 0.5 to 2
- channel_gain: float32 [2048], replicated, may hold values from 0.1 to 1.9
- expand_weight: float32 [2048, 8192], P('fs', 'tp'), may hold values from -0.125 to 0.125
- expand_scale: float32 [8192], P('tp'), may hold values from 0.5 to 2
- reduce_weight: float32 [8192, 2048], P('tp', 'fs'), may hold values from -0.0625 to 0.0625
- reduce_scale: float32 [2048], P('fs'), may hold values from 0.5 to 2
Outputs:
- result: bfloat16 [4096, 2048], P(('rep', 'fs', 'tp'))
Inputs may be any that keep to these rules, and one draw needn't show every extreme that they name: `value_scale`: positive column scales.
All inputs are finite; a program needn't handle non-finite values.
Results may differ from a plain program's by a relative error of at most 0.024.
Values may be sent and summed in bfloat16 or wider, within the bound.
A program may use at most 64 MiB of HBM per device.

v0:
```python
import jax
import jax.numpy as jnp
from jax import lax
from jax.sharding import PartitionSpec as P

GDIM = 64
BLOCK = 128


epsilon = 1e-06


def rms_rows(rows, gain):
    floats = rows.astype(jnp.float32)
    scaled = floats * lax.rsqrt(jnp.mean(floats * floats, axis=-1, keepdims=True) + epsilon)
    return (scaled * gain).astype(jnp.bfloat16)


def body(
    tokens,
    mixer_gain,
    direct_weight,
    direct_scale,
    value_weight,
    value_scale,
    value_gain,
    value_shift,
    spatial_weight,
    spatial_bias,
    merge_weight,
    merge_scale,
    channel_gain,
    expand_weight,
    expand_scale,
    reduce_weight,
    reduce_scale,
):
    direct_half = direct_weight.astype(jnp.bfloat16)
    value_half = value_weight.astype(jnp.bfloat16)
    merge_half = merge_weight.astype(jnp.bfloat16)
    expand_half = expand_weight.astype(jnp.bfloat16)
    reduce_half = reduce_weight.astype(jnp.bfloat16)
    full_expand, full_reduce, reduce_full_scale = (
        lax.all_gather(expand_half, "fs", axis=0, tiled=True),
        lax.all_gather(reduce_half, "fs", axis=1, tiled=True),
        lax.all_gather(reduce_scale.astype(jnp.bfloat16), "fs", axis=0, tiled=True).astype(
            reduce_scale.dtype
        ),
    )
    normed = rms_rows(tokens, mixer_gain)
    whole = lax.all_gather(normed, "tp", axis=0, tiled=True)
    seq_rows = whole.shape[0]
    local_width = direct_weight.shape[1]
    direct_pre = jnp.dot(
        whole,
        lax.all_gather(direct_half, "fs", axis=0, tiled=True),
        preferred_element_type=jnp.float32,
    )
    value_pre = jnp.dot(
        whole,
        lax.all_gather(value_half, "fs", axis=0, tiled=True),
        preferred_element_type=jnp.float32,
    )
    full_merge, merge_full_scale = (
        lax.all_gather(merge_half, "fs", axis=1, tiled=True),
        lax.all_gather(merge_scale.astype(jnp.bfloat16), "fs", axis=0, tiled=True).astype(
            merge_scale.dtype
        ),
    )
    direct = jax.nn.gelu(direct_pre * direct_scale)
    value = jax.nn.gelu(value_pre * value_scale)
    total, squares = lax.psum((jnp.sum(value, axis=1), jnp.sum(value * value, axis=1)), "tp")
    branch_width = local_width * lax.axis_size("tp")
    mean = (total / branch_width)[:, None]
    var = (squares / branch_width)[:, None] - mean * mean
    gated_value = ((value - mean) * lax.rsqrt(var + epsilon) * value_gain + value_shift).astype(
        jnp.bfloat16
    )
    local_groups = spatial_weight.shape[0]
    blocks = gated_value.reshape(seq_rows // BLOCK, BLOCK, local_groups, GDIM)
    mixed = jnp.einsum("gpq,nqgc->npgc", spatial_weight, blocks, preferred_element_type=jnp.float32)
    mixed = mixed + jnp.transpose(spatial_bias)[None, :, :, None]
    gated = (direct * mixed.reshape(seq_rows, local_width)).astype(jnp.bfloat16)
    rows = gated
    mix = lax.psum_scatter(
        (jnp.dot(rows, full_merge, preferred_element_type=jnp.float32) * merge_full_scale).astype(
            jnp.bfloat16
        ),
        "tp",
        scatter_dimension=0,
        tiled=True,
    ).astype(jnp.float32)
    middle = (tokens.astype(jnp.float32) + mix).astype(jnp.bfloat16)
    normed_mid = rms_rows(middle, channel_gain)
    whole_mid = lax.all_gather(normed_mid, "tp", axis=0, tiled=True)
    upper = jnp.dot(whole_mid, full_expand, preferred_element_type=jnp.float32)
    hidden = jnp.square(jax.nn.relu(upper * expand_scale)).astype(jnp.bfloat16)
    rows = hidden
    lower = lax.psum_scatter(
        (jnp.dot(rows, full_reduce, preferred_element_type=jnp.float32) * reduce_full_scale).astype(
            jnp.bfloat16
        ),
        "tp",
        scatter_dimension=0,
        tiled=True,
    ).astype(jnp.float32)
    return (middle.astype(jnp.float32) + lower).astype(jnp.bfloat16)


def solution(mesh):
    return jax.shard_map(
        body,
        mesh=mesh,
        in_specs=(
            P(("rep", "fs", "tp"), None),
            P(),
            P("fs", "tp"),
            P("tp"),
            P("fs", "tp"),
            P("tp"),
            P("tp"),
            P("tp"),
            P("tp", None, None),
            P("tp", None),
            P("tp", "fs"),
            P("fs"),
            P(),
            P("fs", "tp"),
            P("tp"),
            P("tp", "fs"),
            P("fs"),
        ),
        out_specs=P(("rep", "fs", "tp"), None),
        check_vma=False,
    )
```

profile of v0, /device:TPU:0, one launch (start us, length us, event | category | flops | bytes accessed | tf_op | source)
XLA Modules:
  0.0 539.8 jit_solution(16502499518747901413)
XLA Ops:
  6.6 1.8 convert_element_type.71
  8.5 1.2 fusion.1
  9.7 2.0 fusion.3
  11.8 0.0 all-gather.12.cloned.1.call-start
  11.8 1.8 convert_element_type.70
  13.7 0.7 convert_element_type.74
  14.4 0.0 reduce-scatter.3.cloned.1.call-start
  14.5 13.9 %all-gather = bf16[4,1,512]{2,1,0:T(2,128)(2,1)S(1)} all-gather(bf16[1,1,512]{2,1,0:T(2,128)(2,1)S(1)} %reshape.40), channel_id=1, replica_groups=mesh['rep'=2,'fs'=4,'tp'=4] {'fs'}, dimensions={0}, use_global_device_ids=true | all-gather | bytes 5120 | tf_op jit(solution)/shard_map/all_gather | solution.py:66
  28.4 11.3 %all-gather.14.cloned.1.call-done = bf16[2048,256]{1,0:T(8,128)(2,1)} async-done(((bf16[512,256]{1,0:T(8,128)(2,1)}), bf16[2048,256]{1,0:T(8,128)(2,1)}) %all-gather.14.cloned.1.call-update) | async-done | bytes 1048592 | tf_op jit(solution)/shard_map/all_gather | solution.py:61
  39.7 23.5 %all-gather.10.cloned.1.call-done = bf16[512,2048]{1,0:T(8,128)(2,1)} async-done(((bf16[128,2048]{1,0:T(8,128)(2,1)}), bf16[512,2048]{1,0:T(8,128)(2,1)}) %all-gather.10.cloned.1.call-update) | async-done | bytes 2097168 | tf_op jit(solution)/shard_map/all_gather | solution.py:51
  63.3 2.8 fusion.37
  66.1 5.9 %all-reduce = (f32[512]{0:T(512)S(1)}, f32[512]{0:T(512)S(1)}) all-reduce(f32[512]{0:T(512)S(1)} %get-tuple-element.6, f32[512]{0:T(512)S(1)} %get-tuple-element.5), channel_id=1, replica_groups=mesh['rep'=2,'fs'=4,'tp'=4] {'tp'}, use_global_device_ids=true, to_apply=%region_4.0 | all-reduce | flops 1024 | bytes 8192 | tf_op jit(solution)/shard_map/psum | solution.py:72
  72.0 0.2 add_convert_fusion
  72.2 0.2 reshape.47
  72.5 0.3 fusion
  72.8 0.4 copy.35
  73.2 0.6 reshape.48
  73.8 19.1 %all-gather.12.cloned.1.call-done = bf16[2048,256]{1,0:T(8,128)(2,1)} async-done(((bf16[512,256]{1,0:T(8,128)(2,1)}), bf16[2048,256]{1,0:T(8,128)(2,1)}) %all-gather.12.cloned.1.call-update) | async-done | bytes 1048592 | tf_op jit(solution)/shard_map/all_gather | solution.py:56
  92.9 28.8 %all-gather.16.cloned.1.call-done = bf16[256,2048]{1,0:T(8,128)(2,1)} async-done(((bf16[256,512]{1,0:T(8,128)(2,1)}), bf16[256,2048]{1,0:T(8,128)(2,1)}) %all-gather.16.cloned.1.call-update) | async-done | bytes 1048592 | tf_op jit(solution)/shard_map/all_gather | solution.py:65
  121.7 5.9 %multiply_convert_fusion.2 = bf16[512,2048]{1,0:T(8,128)(2,1)} fusion(bf16[256,2048]{1,0:T(8,128)(2,1)} %all-gather.16.cloned.1.call-done, f32[2048]{0:T(1024)S(1)} %bitcast.20, f32[512,256]{1,0:T(8,128)S(1)} %reshape.48, bf16[512,2048]{1,0:T(8,128)(2,1)} %all-gather.10.cloned.1.call-done, bf16[2048,256]{1,0:T(8,128)(2,1)} %all-gather.12.cloned.1.call-done, ...), kind=kOutput, calls=%fused_computation.2 | convolution fusion | flops 1077280768 | bytes 6824960 | tf_op jit(solution)/shard_map/dot_general | solution.py:86
  127.7 30.7 %reduce-scatter.3.cloned.1.call-done = bf16[128,2048]{1,0:T(8,128)(2,1)} async-done(((bf16[512,2048]{1,0:T(8,128)(2,1)}), bf16[128,2048]{1,0:T(8,128)(2,1)}) %reduce-scatter.3.cloned.1.call-update) | async-done | bytes 524304 | tf_op jit(solution)/shard_map/reduce_scatter | solution.py:85
  158.3 1.3 fusion.5
  159.7 2.0 fusion.7
  161.8 3.8 convert_element_type.82
  165.7 3.9 convert_element_type.84
  169.6 12.1 %all-gather.1 = bf16[4,1,512]{2,1,0:T(2,128)(2,1)S(1)} all-gather(bf16[1,1,512]{2,1,0:T(2,128)(2,1)S(1)} %reshape.42), channel_id=1, replica_groups=mesh['rep'=2,'fs'=4,'tp'=4] {'fs'}, dimensions={0}, use_global_device_ids=true | all-gather | bytes 5120 | tf_op jit(solution)/shard_map/all_gather | solution.py:46
  181.8 2.7 all-gather.18.cloned.1.call-done
  184.4 151.2 %all-gather.20.cloned.1.call-done = bf16[2048,2048]{1,0:T(8,128)(2,1)} async-done(((bf16[512,2048]{1,0:T(8,128)(2,1)}), bf16[2048,2048]{1,0:T(8,128)(2,1)}) %all-gather.20.cloned.1.call-update) | async-done | bytes 8388624 | tf_op jit(solution)/shard_map/all_gather | solution.py:44
  335.7 149.4 %all-gather.22.cloned.1.call-done = bf16[2048,2048]{1,0:T(8,128)(2,1)} async-done(((bf16[2048,512]{1,0:T(8,128)(2,1)}), bf16[2048,2048]{1,0:T(8,128)(2,1)}) %all-gather.22.cloned.1.call-update) | async-done | bytes 8388624 | tf_op jit(solution)/shard_map/all_gather | solution.py:45
  485.1 16.6 %multiply_convert_fusion = bf16[512,2048]{1,0:T(8,128)(2,1)} fusion(bf16[2048,2048]{1,0:T(8,128)(2,1)} %all-gather.22.cloned.1.call-done, f32[2048]{0:T(1024)S(1)} %bitcast.21, bf16[512,2048]{1,0:T(8,128)(2,1)} %all-gather.18.cloned.1.call-done, bf16[2048,2048]{1,0:T(8,128)(2,1)} %all-gather.20.cloned.1.call-done, f32[2048]{0:T(1024)S(1)} %copy-done.10), kind=kOutput, calls=%fused_computation | convolution fusion | flops 8596226048 | bytes 20987904 | tf_op jit(solution)/shard_map/dot_general | solution.py:100
  501.6 29.5 %reduce-scatter.5.cloned.1.call-done = bf16[128,2048]{1,0:T(8,128)(2,1)} async-done(((bf16[512,2048]{1,0:T(8,128)(2,1)}), bf16[128,2048]{1,0:T(8,128)(2,1)}) %reduce-scatter.5.cloned.1.call-update) | async-done | bytes 524304 | tf_op jit(solution)/shard_map/reduce_scatter | solution.py:99
  531.2 2.1 fusion.8
  (51 shorter events, 0.6 us)
Async XLA Ops:
  6.5 65.9 %copy-start = (bf16[4,128,128]{2,1,0:T(8,128)(2,1)S(1)}, bf16[4,128,128]{2,1,0:T(8,128)(2,1)}, u32[]{:S(2)}) copy-start(bf16[4,128,128]{2,1,0:T(8,128)(2,1)} %param.25) | copy-start | bytes 393220
  6.5 7.1 %copy-start.3 = (f32[256,512]{1,0:T(8,128)S(1)}, f32[256,512]{1,0:T(8,128)}, u32[]{:S(2)}) copy-start(f32[256,512]{1,0:T(8,128)} %param.27) | copy-start | bytes 1572868
  6.5 7.9 %copy-start.6 = (f32[512]{0:T(512)S(1)}, f32[512]{0:T(512)}, u32[]{:S(2)}) copy-start(f32[512]{0:T(512)} %param.28) | copy-start | bytes 6148
  6.5 56.7 %copy-start.11 = (f32[256]{0:T(256)S(1)}, f32[256]{0:T(256)}, u32[]{:S(2)}) copy-start(f32[256]{0:T(256)} %param.22) | copy-start | bytes 3076
  6.5 33.2 %all-gather.14.cloned.1.call-start = ((), (), s32[]{:S(2)}) async-start(), calls=%async_computation.4 | async-start | bytes 1310720 | tf_op jit(solution)/shard_map/all_gather | solution.py:61
  8.4 54.8 %all-gather.10.cloned.1.call-start = ((), (), s32[]{:S(2)}) async-start(), calls=%async_computation.2 | async-start | bytes 2621440 | tf_op jit(solution)/shard_map/all_gather | solution.py:51
  11.8 81.1 %all-gather.12.cloned.1.call-start = ((), (), s32[]{:S(2)}) async-start(), calls=%async_computation.3 | async-start | bytes 1310720 | tf_op jit(solution)/shard_map/all_gather | solution.py:56
  13.6 108.1 %all-gather.16.cloned.1.call-start = ((), (), s32[]{:S(2)}) async-start(), calls=%async_computation.5 | async-start | bytes 1310720 | tf_op jit(solution)/shard_map/all_gather | solution.py:65
  14.4 57.6 %copy-start.8 = (f32[256]{0:T(256)S(1)}, f32[256]{0:T(256)}, u32[]{:S(2)}) copy-start(f32[256]{0:T(256)} %param.24) | copy-start | bytes 3076
  14.4 57.6 %copy-start.9 = (f32[256]{0:T(256)S(1)}, f32[256]{0:T(256)}, u32[]{:S(2)}) copy-start(f32[256]{0:T(256)} %param.23) | copy-start | bytes 3076
  14.4 143.9 %reduce-scatter.3.cloned.1.call-start = ((), (), s32[]{:S(2)}) async-start(), calls=%async_computation.6 | async-start | bytes 2621440 | tf_op jit(solution)/shard_map/reduce_scatter | solution.py:85
  28.4 44.0 %copy-start.5 = (f32[4,128]{1,0:T(4,128)S(1)}, f32[4,128]{1,0:T(4,128)}, u32[]{:S(2)}) copy-start(f32[4,128]{1,0:T(4,128)} %param.26) | copy-start | bytes 6148
  66.1 55.6 %copy-start.12 = (f32[256]{0:T(256)S(1)}, f32[256]{0:T(256)}, u32[]{:S(2)}) copy-start(f32[256]{0:T(256)} %param.20) | copy-start | bytes 3076
  121.7 36.7 %copy-start.1 = (bf16[128,2048]{1,0:T(8,128)(2,1)S(1)}, bf16[128,2048]{1,0:T(8,128)(2,1)}, u32[]{:S(2)}) copy-start(bf16[128,2048]{1,0:T(8,128)(2,1)} %param.17) | copy-start | bytes 1572868
  121.7 38.0 %copy-start.4 = (f32[2048]{0:T(1024)S(1)}, f32[2048]{0:T(1024)}, u32[]{:S(2)}) copy-start(f32[2048]{0:T(1024)} %param.29) | copy-start | bytes 24580
  127.6 56.8 %all-gather.18.cloned.1.call-start = ((), (), s32[]{:S(2)}) async-start(), calls=%async_computation.7 | async-start | bytes 2621440 | tf_op jit(solution)/shard_map/all_gather | solution.py:95
  161.7 173.9 %all-gather.20.cloned.1.call-start = ((), (), s32[]{:S(2)}) async-start(), calls=%async_computation.8 | async-start | bytes 10485760 | tf_op jit(solution)/shard_map/all_gather | solution.py:44
  165.6 4.0 copy-start.7
  165.6 319.4 %copy-start.10 = (f32[2048]{0:T(1024)S(1)}, f32[2048]{0:T(1024)}, u32[]{:S(2)}) copy-start(f32[2048]{0:T(1024)} %param.31) | copy-start | bytes 24580
  165.6 319.4 %all-gather.22.cloned.1.call-start = ((), (), s32[]{:S(2)}) async-start(), calls=%async_computation.9 | async-start | bytes 10485760 | tf_op jit(solution)/shard_map/all_gather | solution.py:45
  169.6 361.6 %reduce-scatter.5.cloned.1.call-start = ((), (), s32[]{:S(2)}) async-start(), calls=%async_computation.10 | async-start | bytes 2621440 | tf_op jit(solution)/shard_map/reduce_scatter | solution.py:99
  485.0 46.1 %copy-start.2 = (bf16[128,2048]{1,0:T(8,128)(2,1)S(1)}, bf16[128,2048]{1,0:T(8,128)(2,1)}, u32[]{:S(2)}) copy-start(bf16[128,2048]{1,0:T(8,128)(2,1)} %reduce-scatter.3.cloned.1.call-done) | copy-start | bytes 1572868
Sparse Core Ops, SparseCore 0:
  8.9 30.7 all-gather.13
  41.3 21.9 all-gather.9
  64.9 27.9 all-gather.11
  94.3 27.3 all-gather.15
  127.7 30.5 reduce-scatter.2
  161.8 22.5 all-gather.17
  186.0 149.5 all-gather.19
  337.2 147.7 all-gather.21
  501.8 29.3 reduce-scatter.4
where the time goes:
time: 540 us
  waiting for transfers between devices  446 us (83%)
  blocking collectives  31.9 us (6%)
  matrix products  25.6 us (5%)
  other arithmetic  20.9 us (4%)
  between operations  13.4 us (2%)
    all_gather x1, waiting for transfers between devices, body(): lax.all_gather(expand_half, 'fs', axis=0, tiled=True)  151 us
    all_gather x1, waiting for transfers between devices, body(): lax.all_gather(reduce_half, 'fs', axis=1, tiled=True)  149 us
    reduce_scatter x1, waiting for transfers between devices, body(): lax.psum_scatter((jnp.dot(rows, full_merge, preferred_element_type=jnp.fl...  30.7 us
    reduce_scatter x1, waiting for transfers between devices, body(): lax.psum_scatter((jnp.dot(rows, full_reduce, preferred_element_type=jnp.f...  29.5 us
    all_gather x1, waiting for transfers between devices, body(): lax.all_gather(merge_half, 'fs', axis=1, tiled=True)  28.8 us
    all_gather x1, waiting for transfers between devices, body(): whole = lax.all_gather(normed, 'tp', axis=0, tiled=True)  23.5 us
    all_gather x1, waiting for transfers between devices, body(): lax.all_gather(direct_half, 'fs', axis=0, tiled=True)  19.1 us
    dot_general x1, matrix products, body(): jnp.dot(rows, full_reduce, preferred_element_type=jnp.float32)  16.6 us
  transfers between devices with their start and end apart: 9, of which 9 were waited for; matrix products, arithmetic and copies ran while one was open for 3% of the time, Pallas kernels for 0%

commit v1 on v0

--- a/solution.py
+++ b/solution.py
@@ -1,6 +1,8 @@
 import jax
 import jax.numpy as jnp
 from jax import lax
+from jax.experimental import pallas as pl
+from jax.experimental.pallas import tpu as pltpu
 from jax.sharding import PartitionSpec as P
 
 GDIM = 64
@@ -107,9 +109,433 @@
     return (middle.astype(jnp.float32) + lower).astype(jnp.bfloat16)
 
 
+MESH = pl.DeviceIdType.MESH
+
+
+def fused_kernel(
+    tok_ref, mgain_ref, dv_ref, dvscale_ref, vgain_ref, vshift_ref, sw_ref, sbias_ref,
+    mg_ref, cgain_ref, ex_ref, exscale_ref, rd_ref,
+    out_ref,
+    dv_all, mg_all, ex_all, rd_all,
+    xg, act, stat, gated, p1, r1, s1, x1, mid,
+    nm, acc, hid, p2, r2, s2, x2,
+    own_sem, wsend, wrecv, gsend, grecv, tsend, trecv, msend, mrecv, nsend, nrecv, fsend, frecv,
+):
+    rows, width = tok_ref.shape
+    piece = dv_ref.shape[0]
+    local = vgain_ref.shape[1]
+    seq = xg.shape[0]
+    r = lax.axis_index("rep")
+    f = lax.axis_index("fs")
+    t = lax.axis_index("tp")
+    y, c = t // 2, t % 2
+    right, left, across = (f + 1) % 4, (f + 3) % 4, (f + 2) % 4
+    sib = {"tp": y * 2 + (1 - c)}
+    ynb = {"tp": (1 - y) * 2 + c}
+    xnb = {"rep": 1 - r}
+
+    barrier = pltpu.get_barrier_semaphore()
+    for dev in (sib, ynb, xnb, {"fs": right}, {"fs": left}):
+        pl.semaphore_signal(barrier, inc=1, device_id=dev, device_id_type=MESH)
+    pl.semaphore_wait(barrier, 5)
+
+    def rcopy(src, dst, ssem, rsem, dev):
+        return pltpu.make_async_remote_copy(
+            src_ref=src, dst_ref=dst, send_sem=ssem, recv_sem=rsem,
+            device_id=dev, device_id_type=MESH,
+        )
+
+    items = ((dv_ref, dv_all), (mg_ref, mg_all), (ex_ref, ex_all), (rd_ref, rd_all))
+
+    def first(i, d):
+        src, dst = items[i]
+        return rcopy(
+            src, dst.at[f], wsend.at[i, d, 0], wrecv.at[i, d, 0],
+            {"fs": right if d == 0 else left},
+        )
+
+    def relay(i, d):
+        dst = items[i][1]
+        half = dst.shape[1] // 2
+        part = dst.at[left if d == 0 else right, pl.ds(d * half, half)]
+        return rcopy(
+            part, part, wsend.at[i, d, 1], wrecv.at[i, d, 1],
+            {"fs": right if d == 0 else left},
+        )
+
+    def first_start(i):
+        for d in range(2):
+            first(i, d).start()
+
+    def relay_start(i):
+        for d in range(2):
+            first(i, d).wait_recv()
+            relay(i, d).start()
+
+    def relay_wait(i):
+        for d in range(2):
+            relay(i, d).wait_recv()
+
+    first_start(0)
+    first_start(1)
+    owns = [
+        pltpu.make_async_copy(src, dst.at[f], own_sem.at[i])
+        for i, (src, dst) in enumerate(items)
+    ]
+    for own in owns:
+        own.start()
+
+    def norm(x, gain):
+        return (
+            x * lax.rsqrt(jnp.mean(x * x, axis=-1, keepdims=True) + epsilon) * gain
+        ).astype(jnp.bfloat16)
+
+    def block(n, size=1):
+        return pl.ds(pl.multiple_of(n * rows, rows), size * rows)
+
+    def columns(slot):
+        return pl.ds(pl.multiple_of(slot * piece, piece), piece)
+
+    mine = xg.at[block(c * 2 + y)]
+    mine[...] = norm(tok_ref[...].astype(jnp.float32), mgain_ref[...])
+    far = xg.at[block(c * 2 + 1 - y)]
+    gather = (
+        rcopy(mine, mine, gsend.at[0], grecv.at[0], sib),
+        rcopy(mine, mine, gsend.at[1], grecv.at[1], ynb),
+        rcopy(far, far, gsend.at[2], grecv.at[2], sib),
+    )
+    gather[1].start()
+    gather[0].start()
+    gather[1].wait_recv()
+    gather[2].start()
+    relay_start(0)
+    relay_start(1)
+    first_start(2)
+    first_start(3)
+    gather[0].wait_recv()
+    gather[2].wait_recv()
+    for own in owns:
+        own.wait()
+
+    def project(slot):
+        return jnp.dot(xg[:, columns(slot)], dv_all[slot], preferred_element_type=jnp.float32)
+
+    act[...] = project(f)
+    act[...] += project(left)
+    act[...] += project(right)
+    relay_wait(0)
+    act[...] = jax.nn.gelu((act[...] + project(across)) * dvscale_ref[...])
+
+    lane = lax.broadcasted_iota(jnp.int32, (rows, rows), 1)
+    for n in range(4):
+        value = act[n * rows : (n + 1) * rows, local:]
+        total = jnp.sum(value, axis=1, keepdims=True)
+        squares = jnp.sum(value * value, axis=1, keepdims=True)
+        table = jnp.where(lane == 0, total, jnp.where(lane == 1, squares, 0.0))
+        stat[t, n] = jnp.transpose(table)[:8]
+    stats = [
+        rcopy(stat.at[t], stat.at[t], tsend.at[0], trecv.at[0], sib),
+        rcopy(stat.at[t], stat.at[t], tsend.at[1], trecv.at[1], ynb),
+        rcopy(
+            stat.at[(1 - y) * 2 + c], stat.at[(1 - y) * 2 + c], tsend.at[2], trecv.at[2], sib
+        ),
+    ]
+    stats[1].start()
+    stats[0].start()
+    stats[1].wait_recv()
+    stats[2].start()
+    stats[0].wait_recv()
+    stats[2].wait_recv()
+    inverse = 1.0 / (local * 4)
+    group_lane = lax.broadcasted_iota(jnp.int32, (rows, 128), 1) // GDIM
+    for n in range(4):
+        here = slice(n * rows, (n + 1) * rows)
+        summed = stat[0, n] + stat[1, n] + stat[2, n] + stat[3, n]
+        table = jnp.transpose(jnp.concatenate([summed] * (rows // 8), axis=0))
+        mean = table[:, 0:1] * inverse
+        var = table[:, 1:2] * inverse - mean * mean
+        gv = (
+            (act[here, local:] - mean) * lax.rsqrt(var + epsilon) * vgain_ref[...]
+            + vshift_ref[...]
+        ).astype(jnp.bfloat16)
+        per = 128 // GDIM
+        for j in range(local // 128):
+            at = slice(j * 128, (j + 1) * 128)
+            mixed = jnp.dot(sw_ref[j * per], gv[:, at], preferred_element_type=jnp.float32)
+            for k in range(1, per):
+                other = jnp.dot(
+                    sw_ref[j * per + k], gv[:, at], preferred_element_type=jnp.float32
+                )
+                mixed = jnp.where(group_lane == k, other, mixed)
+            gated[here, at] = (act[here, at] * (mixed + sbias_ref[:, at])).astype(jnp.bfloat16)
+
+    slots = (f, left, right, across)
+
+    def merge_pair(k):
+        return rcopy(
+            p1.at[k, block((1 - c) * 2, 2)], r1.at[k], msend.at[k, 0], mrecv.at[k, 0], sib
+        )
+
+    def merge_far(k):
+        return rcopy(s1.at[k], x1.at[k], msend.at[k, 1], mrecv.at[k, 1], ynb)
+
+    def merge_send(k):
+        merge_pair(k).wait_recv()
+        s1[k] = (
+            p1[k, block(c * 2 + 1 - y)].astype(jnp.float32)
+            + r1[k, block(1 - y)].astype(jnp.float32)
+        ).astype(jnp.bfloat16)
+        merge_far(k).start()
+
+    for k, slot in enumerate(slots):
+        if k == 3:
+            relay_wait(1)
+        p1[k] = jnp.dot(gated[...], mg_all[slot], preferred_element_type=jnp.float32).astype(
+            jnp.bfloat16
+        )
+        merge_pair(k).start()
+        if k > 0:
+            merge_send(k - 1)
+    merge_send(3)
+    for k, slot in enumerate(slots):
+        merge_far(k).wait_recv()
+        mid[:, columns(slot)] = (
+            tok_ref[:, columns(slot)].astype(jnp.float32)
+            + p1[k, block(c * 2 + y)].astype(jnp.float32)
+            + r1[k, block(y)].astype(jnp.float32)
+            + x1[k].astype(jnp.float32)
+        ).astype(jnp.bfloat16)
+
+    def place(rr, yy):
+        return nm.at[block(c * 4 + rr * 2 + yy)]
+
+    half = rows // 2
+    mine = place(r, y)
+    mine[...] = norm(mid[...].astype(jnp.float32), cgain_ref[...])
+    from_x, from_y, from_xy = place(1 - r, y), place(r, 1 - y), place(1 - r, 1 - y)
+    low, high = from_x.at[pl.ds(0, half)], from_y.at[pl.ds(half, half)]
+    spread = (
+        rcopy(mine, mine, nsend.at[0], nrecv.at[0], xnb),
+        rcopy(mine, mine, nsend.at[1], nrecv.at[1], ynb),
+        rcopy(mine, mine, nsend.at[2], nrecv.at[2], sib),
+        rcopy(low, low, nsend.at[3], nrecv.at[3], ynb),
+        rcopy(high, high, nsend.at[4], nrecv.at[4], xnb),
+        rcopy(from_x, from_x, nsend.at[5], nrecv.at[5], sib),
+        rcopy(from_y, from_y, nsend.at[6], nrecv.at[6], sib),
+        rcopy(from_xy, from_xy, nsend.at[7], nrecv.at[7], sib),
+    )
+    for k in range(3):
+        spread[k].start()
+    relay_start(2)
+    spread[0].wait_recv()
+    spread[3].start()
+    spread[5].start()
+    spread[1].wait_recv()
+    spread[4].start()
+    spread[6].start()
+    relay_start(3)
+    spread[3].wait_recv()
+    spread[4].wait_recv()
+    spread[7].start()
+    for k in (2, 5, 6, 7):
+        spread[k].wait_recv()
+
+    everyone = nm.shape[0]
+    tall = 2 * rows
+
+    def over_rows(step):
+        lax.fori_loop(
+            0, everyone // tall,
+            lambda i, _: step(pl.ds(pl.multiple_of(i * tall, tall), tall)), None,
+        )
+
+    def expand(at, slot):
+        return jnp.dot(nm[at, columns(slot)], ex_all[slot], preferred_element_type=jnp.float32)
+
+    def expand_most(at):
+        acc[at] = expand(at, f) + expand(at, left) + expand(at, right)
+
+    def expand_last(at):
+        upper = (acc[at] + expand(at, across)) * exscale_ref[...]
+        hid[at] = jnp.square(jax.nn.relu(upper)).astype(jnp.bfloat16)
+
+    over_rows(expand_most)
+    relay_wait(2)
+    over_rows(expand_last)
+
+    def down_pair(k):
+        return rcopy(
+            p2.at[k, block((1 - c) * 4, 4)], r2.at[k], fsend.at[k, 0], frecv.at[k, 0], sib
+        )
+
+    hops = ((1 - r, y), (r, 1 - y), (1 - r, 1 - y))
+
+    def down_far(k, h):
+        rr, yy = hops[h]
+        dev = (xnb, ynb)[h]
+        return rcopy(
+            s2.at[k, block(rr * 2 + yy)], x2.at[k, h], fsend.at[k, 1 + h], frecv.at[k, 1 + h], dev
+        )
+
+    def down_via(k, h):
+        return rcopy(
+            s2.at[k, pl.ds(pl.multiple_of((hops[2][0] * 2 + hops[2][1]) * rows + h * half, half), half)],
+            x2.at[k, 2, pl.ds(h * half, half)],
+            fsend.at[k, 3 + h], frecv.at[k, 3 + h], (xnb, ynb)[h],
+        )
+
+    def down_on(k, h):
+        return rcopy(
+            x2.at[k, 2, pl.ds(h * half, half)], x2.at[k, 3, pl.ds(h * half, half)],
+            fsend.at[k, 5 + h], frecv.at[k, 5 + h], (ynb, xnb)[h],
+        )
+
+    def down_send(k):
+        down_pair(k).wait_recv()
+        s2[k] = (
+            p2[k, block(c * 4, 4)].astype(jnp.float32) + r2[k].astype(jnp.float32)
+        ).astype(jnp.bfloat16)
+        for h in range(2):
+            down_via(k, h).start()
+        for h in range(2):
+            down_far(k, h).start()
+
+    def down_relay(k):
+        for h in range(2):
+            down_via(k, h).wait_recv()
+            down_on(k, h).start()
+
+    for k, slot in enumerate(slots):
+        if k == 3:
+            relay_wait(3)
+
+        def reduce(at, k=k, slot=slot):
+            p2[k, at] = jnp.dot(
+                hid[at], rd_all[slot], preferred_element_type=jnp.float32
+            ).astype(jnp.bfloat16)
+
+        over_rows(reduce)
+        down_pair(k).start()
+        if k > 0:
+            down_send(k - 1)
+        if k > 1:
+            down_relay(k - 2)
+    down_send(3)
+    down_relay(2)
+    down_relay(3)
+    for k, slot in enumerate(slots):
+        for h in range(2):
+            down_far(k, h).wait_recv()
+            down_on(k, h).wait_recv()
+        out_ref[:, columns(slot)] = (
+            mid[:, columns(slot)].astype(jnp.float32)
+            + p2[k, block(c * 4 + r * 2 + y)].astype(jnp.float32)
+            + r2[k, block(r * 2 + y)].astype(jnp.float32)
+            + x2[k, 0].astype(jnp.float32)
+            + x2[k, 1].astype(jnp.float32)
+            + x2[k, 3].astype(jnp.float32)
+        ).astype(jnp.bfloat16)
+
+    for i in range(4):
+        for d in range(2):
+            first(i, d).wait_send()
+            relay(i, d).wait_send()
+    for copy in gather + tuple(stats) + spread:
+        copy.wait_send()
+    for k in range(4):
+        merge_pair(k).wait_send()
+        merge_far(k).wait_send()
+        down_pair(k).wait_send()
+        for h in range(2):
+            down_far(k, h).wait_send()
+            down_via(k, h).wait_send()
+            down_on(k, h).wait_send()
+
+
+def fused_body(
+    tokens,
+    mixer_gain,
+    direct_weight,
+    direct_scale,
+    value_weight,
+    value_scale,
+    value_gain,
+    value_shift,
+    spatial_weight,
+    spatial_bias,
+    merge_weight,
+    merge_scale,
+    channel_gain,
+    expand_weight,
+    expand_scale,
+    reduce_weight,
+    reduce_scale,
+):
+    bf = jnp.bfloat16
+    rows, width = tokens.shape
+    piece, local = direct_weight.shape
+    wide = expand_weight.shape[1] // 2
+    r = lax.axis_index("rep")
+    dv = jnp.concatenate([direct_weight.astype(bf), value_weight.astype(bf)], axis=1)
+    dvscale = jnp.concatenate([direct_scale, value_scale])[None]
+    sbias = jnp.repeat(jnp.transpose(spatial_bias), GDIM, axis=1)
+    mg = (merge_weight * merge_scale).astype(bf)
+    ex = lax.dynamic_slice_in_dim(expand_weight, r * wide, wide, 1).astype(bf)
+    exscale = lax.dynamic_slice_in_dim(expand_scale, r * wide, wide, 0)[None]
+    rd = (lax.dynamic_slice_in_dim(reduce_weight, r * wide, wide, 0) * reduce_scale).astype(bf)
+    seq = 4 * rows
+    vm = pltpu.VMEM
+    dma = pltpu.SemaphoreType.DMA
+    f32 = jnp.float32
+    operands = (
+        tokens, mixer_gain[None], dv, dvscale, value_gain[None], value_shift[None],
+        spatial_weight, sbias, mg, channel_gain[None], ex, exscale, rd,
+    )
+    return pl.pallas_call(
+        fused_kernel,
+        out_shape=jax.ShapeDtypeStruct((rows, width), bf),
+        in_specs=[pl.BlockSpec(memory_space=pltpu.VMEM)] * len(operands),
+        out_specs=pl.BlockSpec(memory_space=pltpu.VMEM),
+        scratch_shapes=[
+            vm((4, piece, 2 * local), bf),
+            vm((4, local, piece), bf),
+            vm((4, piece, wide), bf),
+            vm((4, wide, piece), bf),
+            vm((seq, width), bf),
+            vm((seq, 2 * local), f32),
+            vm((4, 4, 8, rows), f32),
+            vm((seq, local), bf),
+            vm((4, seq, piece), bf),
+            vm((4, 2 * rows, piece), bf),
+            vm((4, rows, piece), bf),
+            vm((4, rows, piece), bf),
+            vm((rows, width), bf),
+            vm((2 * seq, width), bf),
+            vm((2 * seq, wide), f32),
+            vm((2 * seq, wide), bf),
+            vm((4, 2 * seq, piece), bf),
+            vm((4, seq, piece), bf),
+            vm((4, seq, piece), bf),
+            vm((4, 4, rows, piece), bf),
+            dma((4,)),
+            dma((4, 2, 2)), dma((4, 2, 2)),
+            dma((3,)), dma((3,)),
+            dma((3,)), dma((3,)),
+            dma((4, 2)), dma((4, 2)),
+            dma((8,)), dma((8,)),
+            dma((4, 7)), dma((4, 7)),
+        ],
+        compiler_params=pltpu.CompilerParams(
+            collective_id=0, has_side_effects=True, vmem_limit_bytes=60 * 1024 * 1024
+        ),
+    )(*operands)
+
+
 def solution(mesh):
+    sizes = mesh.shape
+    fused = sizes["rep"] == 2 and sizes["fs"] == 4 and sizes["tp"] == 4
     return jax.shard_map(
-        body,
+        fused_body if fused else body,
         mesh=mesh,
         in_specs=(
             P(("rep", "fs", "tp"), None),

time: 540 us -> 226 us (0.42)
  waiting for transfers between devices: 446 us -> 0 us
  Pallas kernels: 0 us -> 211 us
  blocking collectives: 31.9 us -> 0 us
  matrix products: 25.6 us -> 0 us
  between operations: 13.4 us -> 0.02 us
  other arithmetic: 20.9 us -> 7.72 us
  local copies, waits for them, and re-layouts: 1.32 us -> 7.34 us
    all_gather x7 -> x0, waiting for transfers between devices: 386 us -> none  [the longest x1 151 us: body(): lax.all_gather(expand_half, 'fs', axis=0, tiled=True)]
    pallas_call x0 -> x1, Pallas kernels: none -> 211 us  [fused_body(): pl.pallas_call(fused_kernel, out_shape=jax.ShapeDtypeStruct((rows, width)...]
    reduce_scatter x2 -> x0, waiting for transfers between devices: 60.2 us -> none  [the longest x1 30.7 us: body(): lax.psum_scatter((jnp.dot(rows, full_merge, preferred_element_type=jnp.fl...]
    all_gather x2 -> x0, blocking collectives: 26 us -> none  [the longest x1 13.9 us: body(): lax.all_gather(merge_scale.astype(jnp.bfloat16), 'fs', axis=0, tiled=True)]
    dot_general x4 -> x0, matrix products: 25.6 us -> none  [the longest x1 16.6 us: body(): jnp.dot(rows, full_reduce, preferred_element_type=jnp.float32)]
    convert_element_type x13 -> x4, other arithmetic: 18.4 us -> 5.59 us  [the longest x1 1.79 us: fused_body(): mg = (merge_weight * merge_scale).astype(bf)]
    psum x1 -> x0, blocking collectives: 5.89 us -> none  [body(): lax.psum((jnp.sum(value, axis=1), jnp.sum(value * value, axis=1)), 'tp')]
  transfers between devices with their start and end apart: 9 -> 0, of which waited for: 9 -> 0; matrix products, arithmetic and copies ran while one was open for 3% -> 0% of each run, Pallas kernels for 0% -> 0%
where the time goes in v1:
time: 226 us
  Pallas kernels  211 us (93%)
  other arithmetic  7.72 us (3%)
  local copies, waits for them, and re-layouts  7.34 us (3%)
    pallas_call x1, Pallas kernels, fused_body(): pl.pallas_call(fused_kernel, out_shape=jax.ShapeDtypeStruct((rows, width)...  211 us

profile of v1, /device:TPU:0, one launch (start us, length us, event | category | flops | bytes accessed | tf_op | source)
XLA Modules:
  0.0 225.7 jit_solution(15063033312577931748)
XLA Ops:
  0.0 0.0 copy-start.1
  0.0 1.3 pad_maximum_fusion.1
  1.3 1.3 dynamic_slice.10
  2.6 0.7 broadcast_in_dim.27
  3.3 0.8 copy.19.sbias_ref
  4.0 0.0 copy-start
  4.0 1.2 convert_element_type.15
  5.3 1.3 convert_element_type.16
  6.5 0.8 pad_maximum_fusion.dv_ref
  7.4 1.8 multiply_convert_fusion.1.mg_ref
  9.1 2.7 %dynamic-slice_convert_fusion.ex_ref = bf16[512,1024]{1,0:T(8,128)(2,1)} fusion(f32[512,2048]{1,0:T(8,128)} %param.30, s32[]{:T(128)S(6)} %select_n.2), kind=kLoop, calls=%fused_computation.1 | loop fusion | bytes 2097156 | tf_op jit(solution)/shard_map/convert_element_type | solution.py:483
  11.9 0.0 copy-done.1
  11.9 0.0 copy-done
  11.9 1.3 multiply_convert_fusion.rd_ref
  13.2 210.6 %shard_map.163 = bf16[128,2048]{1,0:T(8,128)(2,1)} custom-call(bf16[128,2048]{1,0:T(8,128)(2,1)} %tok_ref.1, f32[1,2048]{1,0:T(1,128)} %bitcast.10, bf16[512,512]{1,0:T(8,128)(2,1)} %pad_maximum_fusion.dv_ref, f32[1,512]{1,0:T(1,128)} %bitcast.12, f32[1,256]{1,0:T(1,128)} %bitcast.14, f32[1,256]{1,0:T(1,128)} %bitcast.15, bf16[4,128,128]{2,1,0:T(8,128)(2,1)} %sw_ref.1, ...), custom_call_target="tpu_custom_call" | custom-call | tf_op jit(solution)/shard_map/pallas_call | solution.py:494
  223.8 1.9 copy.21
Async XLA Ops:
  0.0 11.9 %copy-start.1 = (f32[512]{0:T(512)S(1)}, f32[512]{0:T(512)}, u32[]{:S(2)}) copy-start(f32[512]{0:T(512)} %param.33) | copy-start | bytes 6148
  4.0 7.9 %copy-start = (f32[2048,512]{1,0:T(8,128)S(1)}, f32[2048,512]{1,0:T(8,128)}, u32[]{:S(2)}) copy-start(f32[2048,512]{1,0:T(8,128)} %param.32) | copy-start | bytes 12582916

commit v2 on v1

--- a/solution.py
+++ b/solution.py
@@ -118,8 +118,8 @@
     out_ref,
     dv_all, mg_all, ex_all, rd_all,
     xg, act, stat, gated, p1, r1, s1, x1, mid,
-    nm, acc, hid, p2, r2, s2, x2,
-    own_sem, wsend, wrecv, gsend, grecv, tsend, trecv, msend, mrecv, nsend, nrecv, fsend, frecv,
+    nm, acc, hid, p2, r2, s2, z2, s3, x2,
+    own_sem, wsend, wrecv, xsend, xrecv, gsend, grecv, tsend, trecv, msend, mrecv, nsend, nrecv, fsend, frecv,
 ):
     rows, width = tok_ref.shape
     piece = dv_ref.shape[0]
@@ -129,15 +129,18 @@
     f = lax.axis_index("fs")
     t = lax.axis_index("tp")
     y, c = t // 2, t % 2
-    right, left, across = (f + 1) % 4, (f + 3) % 4, (f + 2) % 4
+    z = f % 2
+    mate = f + 1 - 2 * z
+    peers = (mate, (f + 2) % 4, (mate + 2) % 4)
     sib = {"tp": y * 2 + (1 - c)}
     ynb = {"tp": (1 - y) * 2 + c}
     xnb = {"rep": 1 - r}
+    znb = {"fs": mate}
 
     barrier = pltpu.get_barrier_semaphore()
-    for dev in (sib, ynb, xnb, {"fs": right}, {"fs": left}):
+    for dev in (sib, ynb, xnb) + tuple({"fs": peer} for peer in peers):
         pl.semaphore_signal(barrier, inc=1, device_id=dev, device_id_type=MESH)
-    pl.semaphore_wait(barrier, 5)
+    pl.semaphore_wait(barrier, 6)
 
     def rcopy(src, dst, ssem, rsem, dev):
         return pltpu.make_async_remote_copy(
@@ -145,42 +148,51 @@
             device_id=dev, device_id_type=MESH,
         )
 
-    items = ((dv_ref, dv_all), (mg_ref, mg_all), (ex_ref, ex_all), (rd_ref, rd_all))
-
-    def first(i, d):
-        src, dst = items[i]
+    mixer = ((dv_ref, dv_all), (mg_ref, mg_all))
+
+    def part(i, slot, q):
+        ref = mixer[i][1]
+        size = ref.shape[1] // 2
+        return ref.at[slot, pl.ds(pl.multiple_of(q * size, size), size)]
+
+    def along(i, j):
+        src = mixer[i][0]
+        size = src.shape[0] // 2
         return rcopy(
-            src, dst.at[f], wsend.at[i, d, 0], wrecv.at[i, d, 0],
-            {"fs": right if d == 0 else left},
-        )
-
-    def relay(i, d):
-        dst = items[i][1]
-        half = dst.shape[1] // 2
-        part = dst.at[left if d == 0 else right, pl.ds(d * half, half)]
-        return rcopy(
-            part, part, wsend.at[i, d, 1], wrecv.at[i, d, 1],
-            {"fs": right if d == 0 else left},
-        )
-
-    def first_start(i):
-        for d in range(2):
-            first(i, d).start()
-
-    def relay_start(i):
-        for d in range(2):
-            first(i, d).wait_recv()
-            relay(i, d).start()
-
-    def relay_wait(i):
-        for d in range(2):
-            relay(i, d).wait_recv()
-
-    first_start(0)
-    first_start(1)
+            src.at[pl.ds(pl.multiple_of(r * size, size), size)], part(i, f, r),
+            wsend.at[i, j], wrecv.at[i, j], {"fs": peers[j]},
+        )
+
+    def over(i, j):
+        here = part(i, peers[j], r)
+        return rcopy(here, here, xsend.at[i, j], xrecv.at[i, j], xnb)
+
+    def over_start(i):
+        for j in range(3):
+            along(i, j).wait_recv()
+            over(i, j).start()
+
+    def over_wait(i):
+        for j in range(3):
+            over(i, j).wait_recv()
+
+    def chunk(i, j):
+        to = peers[j] % 2
+        src = ex_ref.at[to] if i == 2 else rd_ref.at[to, i - 3]
+        dst = ex_all.at[f] if i == 2 else rd_all.at[f, i - 3]
+        return rcopy(src, dst, wsend.at[i, j], wrecv.at[i, j], {"fs": peers[j]})
+
+    for i in range(2):
+        for j in range(3):
+            along(i, j).start()
+    for i in range(2, 5):
+        for j in range(3):
+            chunk(i, j).start()
     owns = [
         pltpu.make_async_copy(src, dst.at[f], own_sem.at[i])
-        for i, (src, dst) in enumerate(items)
+        for i, (src, dst) in enumerate(
+            mixer + ((ex_ref.at[z], ex_all), (rd_ref.at[z], rd_all))
+        )
     ]
     for own in owns:
         own.start()
@@ -208,10 +220,8 @@
     gather[0].start()
     gather[1].wait_recv()
     gather[2].start()
-    relay_start(0)
-    relay_start(1)
-    first_start(2)
-    first_start(3)
+    over_start(0)
+    over_start(1)
     gather[0].wait_recv()
     gather[2].wait_recv()
     for own in owns:
@@ -220,11 +230,11 @@
     def project(slot):
         return jnp.dot(xg[:, columns(slot)], dv_all[slot], preferred_element_type=jnp.float32)
 
+    over_wait(0)
     act[...] = project(f)
-    act[...] += project(left)
-    act[...] += project(right)
-    relay_wait(0)
-    act[...] = jax.nn.gelu((act[...] + project(across)) * dvscale_ref[...])
+    for peer in peers:
+        act[...] += project(peer)
+    act[...] = jax.nn.gelu(act[...] * dvscale_ref[...])
 
     lane = lax.broadcasted_iota(jnp.int32, (rows, rows), 1)
     for n in range(4):
@@ -269,7 +279,7 @@
                 mixed = jnp.where(group_lane == k, other, mixed)
             gated[here, at] = (act[here, at] * (mixed + sbias_ref[:, at])).astype(jnp.bfloat16)
 
-    slots = (f, left, right, across)
+    slots = (f,) + peers
 
     def merge_pair(k):
         return rcopy(
@@ -288,8 +298,8 @@
         merge_far(k).start()
 
     for k, slot in enumerate(slots):
-        if k == 3:
-            relay_wait(1)
+        if k == 1:
+            over_wait(1)
         p1[k] = jnp.dot(gated[...], mg_all[slot], preferred_element_type=jnp.float32).astype(
             jnp.bfloat16
         )
@@ -306,39 +316,47 @@
             + x1[k].astype(jnp.float32)
         ).astype(jnp.bfloat16)
 
-    def place(rr, yy):
-        return nm.at[block(c * 4 + rr * 2 + yy)]
+    def place(zz, rr, yy):
+        return nm.at[block(c * 8 + zz * 4 + rr * 2 + yy)]
 
     half = rows // 2
-    mine = place(r, y)
+    mine = place(z, r, y)
     mine[...] = norm(mid[...].astype(jnp.float32), cgain_ref[...])
-    from_x, from_y, from_xy = place(1 - r, y), place(r, 1 - y), place(1 - r, 1 - y)
-    low, high = from_x.at[pl.ds(0, half)], from_y.at[pl.ds(half, half)]
-    spread = (
-        rcopy(mine, mine, nsend.at[0], nrecv.at[0], xnb),
-        rcopy(mine, mine, nsend.at[1], nrecv.at[1], ynb),
-        rcopy(mine, mine, nsend.at[2], nrecv.at[2], sib),
-        rcopy(low, low, nsend.at[3], nrecv.at[3], ynb),
-        rcopy(high, high, nsend.at[4], nrecv.at[4], xnb),
-        rcopy(from_x, from_x, nsend.at[5], nrecv.at[5], sib),
-        rcopy(from_y, from_y, nsend.at[6], nrecv.at[6], sib),
-        rcopy(from_xy, from_xy, nsend.at[7], nrecv.at[7], sib),
-    )
+    over_fs = rcopy(mine, mine, nsend.at[16], nrecv.at[16], znb)
+
+    def spreading(b, zz):
+        here = place(zz, r, y)
+        from_x, from_y = place(zz, 1 - r, y), place(zz, r, 1 - y)
+        from_xy = place(zz, 1 - r, 1 - y)
+        low, high = from_x.at[pl.ds(0, half)], from_y.at[pl.ds(half, half)]
+        routes = (
+            (here, xnb), (here, ynb), (here, sib), (low, ynb), (high, xnb),
+            (from_x, sib), (from_y, sib), (from_xy, sib),
+        )
+        return tuple(
+            rcopy(ref, ref, nsend.at[8 * b + k], nrecv.at[8 * b + k], dev)
+            for k, (ref, dev) in enumerate(routes)
+        )
+
+    near, far = spreading(0, z), spreading(1, 1 - z)
+    over_fs.start()
     for k in range(3):
-        spread[k].start()
-    relay_start(2)
-    spread[0].wait_recv()
-    spread[3].start()
-    spread[5].start()
-    spread[1].wait_recv()
-    spread[4].start()
-    spread[6].start()
-    relay_start(3)
-    spread[3].wait_recv()
-    spread[4].wait_recv()
-    spread[7].start()
-    for k in (2, 5, 6, 7):
-        spread[k].wait_recv()
+        near[k].start()
+    over_fs.wait_recv()
+    for k in range(3):
+        far[k].start()
+    for spread in (near, far):
+        for k in range(2):
+            spread[k].wait_recv()
+            spread[3 + k].start()
+            spread[5 + k].start()
+    for spread in (near, far):
+        spread[3].wait_recv()
+        spread[4].wait_recv()
+        spread[7].start()
+    for spread in (near, far):
+        for k in (2, 5, 6, 7):
+            spread[k].wait_recv()
 
     everyone = nm.shape[0]
     tall = 2 * rows
@@ -353,20 +371,35 @@
         return jnp.dot(nm[at, columns(slot)], ex_all[slot], preferred_element_type=jnp.float32)
 
     def expand_most(at):
-        acc[at] = expand(at, f) + expand(at, left) + expand(at, right)
+        acc[at] = expand(at, f) + expand(at, peers[0])
 
     def expand_last(at):
-        upper = (acc[at] + expand(at, across)) * exscale_ref[...]
+        upper = (acc[at] + expand(at, peers[1]) + expand(at, peers[2])) * exscale_ref[...]
         hid[at] = jnp.square(jax.nn.relu(upper)).astype(jnp.bfloat16)
 
+    chunk(2, 0).wait_recv()
     over_rows(expand_most)
-    relay_wait(2)
+    chunk(2, 1).wait_recv()
+    chunk(2, 2).wait_recv()
     over_rows(expand_last)
 
     def down_pair(k):
         return rcopy(
-            p2.at[k, block((1 - c) * 4, 4)], r2.at[k], fsend.at[k, 0], frecv.at[k, 0], sib
-        )
+            p2.at[k, block((1 - c) * 8, 8)], r2.at[k], fsend.at[k, 0], frecv.at[k, 0], sib
+        )
+
+    def down_fs(k):
+        return rcopy(
+            s2.at[k], z2.at[k], fsend.at[k, 7], frecv.at[k, 7], znb
+        )
+
+    def down_fs_send(k):
+        down_pair(k).wait_recv()
+        s2[k] = (
+            p2[k, block(c * 8 + (1 - z) * 4, 4)].astype(jnp.float32)
+            + r2[k, block((1 - z) * 4, 4)].astype(jnp.float32)
+        ).astype(jnp.bfloat16)
+        down_fs(k).start()
 
     hops = ((1 - r, y), (r, 1 - y), (1 - r, 1 - y))
 
@@ -374,12 +407,12 @@
         rr, yy = hops[h]
         dev = (xnb, ynb)[h]
         return rcopy(
-            s2.at[k, block(rr * 2 + yy)], x2.at[k, h], fsend.at[k, 1 + h], frecv.at[k, 1 + h], dev
+            s3.at[k, block(rr * 2 + yy)], x2.at[k, h], fsend.at[k, 1 + h], frecv.at[k, 1 + h], dev
         )
 
     def down_via(k, h):
         return rcopy(
-            s2.at[k, pl.ds(pl.multiple_of((hops[2][0] * 2 + hops[2][1]) * rows + h * half, half), half)],
+            s3.at[k, pl.ds(pl.multiple_of((hops[2][0] * 2 + hops[2][1]) * rows + h * half, half), half)],
             x2.at[k, 2, pl.ds(h * half, half)],
             fsend.at[k, 3 + h], frecv.at[k, 3 + h], (xnb, ynb)[h],
         )
@@ -391,9 +424,11 @@
         )
 
     def down_send(k):
-        down_pair(k).wait_recv()
-        s2[k] = (
-            p2[k, block(c * 4, 4)].astype(jnp.float32) + r2[k].astype(jnp.float32)
+        down_fs(k).wait_recv()
+        s3[k] = (
+            p2[k, block(c * 8 + z * 4, 4)].astype(jnp.float32)
+            + r2[k, block(z * 4, 4)].astype(jnp.float32)
+            + z2[k].astype(jnp.float32)
         ).astype(jnp.bfloat16)
         for h in range(2):
             down_via(k, h).start()
@@ -405,47 +440,70 @@
             down_via(k, h).wait_recv()
             down_on(k, h).start()
 
-    for k, slot in enumerate(slots):
-        if k == 3:
-            relay_wait(3)
-
-        def reduce(at, k=k, slot=slot):
-            p2[k, at] = jnp.dot(
-                hid[at], rd_all[slot], preferred_element_type=jnp.float32
-            ).astype(jnp.bfloat16)
-
-        over_rows(reduce)
-        down_pair(k).start()
-        if k > 0:
-            down_send(k - 1)
-        if k > 1:
-            down_relay(k - 2)
-    down_send(3)
-    down_relay(2)
-    down_relay(3)
-    for k, slot in enumerate(slots):
+    steps = ((0, 0), (1, 0), (0, 1), (1, 1), (2, 0), (3, 0), (2, 1), (3, 1))
+    base = f - z
+    order = (base, base + 1, 2 - base, 3 - base)
+
+    def arrived(side, j):
+        rcopy(
+            rd_ref.at[0, side], rd_all.at[f, side],
+            wsend.at[3 + side, j], wrecv.at[3 + side, j], znb,
+        ).wait_recv()
+
+    last = len(steps)
+    thin = piece // 2
+
+    for k in range(last + 3):
+        if k < last:
+            from_slot, side = steps[k]
+            slot = order[from_slot]
+            if from_slot == 0:
+                arrived(side, 0)
+            elif from_slot > 1:
+                arrived(side, 1 + (from_slot + z) % 2)
+
+            def reduce(at, k=k, slot=slot, side=side):
+                p2[k, at] = jnp.dot(
+                    hid[at], rd_all[slot, side], preferred_element_type=jnp.float32
+                ).astype(jnp.bfloat16)
+
+            over_rows(reduce)
+            down_pair(k).start()
+        if 0 < k <= last:
+            down_fs_send(k - 1)
+        if 1 < k <= last + 1:
+            down_send(k - 2)
+        if 2 < k:
+            down_relay(k - 3)
+    for k, (from_slot, side) in enumerate(steps):
         for h in range(2):
             down_far(k, h).wait_recv()
             down_on(k, h).wait_recv()
-        out_ref[:, columns(slot)] = (
-            mid[:, columns(slot)].astype(jnp.float32)
-            + p2[k, block(c * 4 + r * 2 + y)].astype(jnp.float32)
-            + r2[k, block(r * 2 + y)].astype(jnp.float32)
+        at = pl.ds(pl.multiple_of(order[from_slot] * piece + side * thin, thin), thin)
+        out_ref[:, at] = (
+            mid[:, at].astype(jnp.float32)
+            + p2[k, block(c * 8 + z * 4 + r * 2 + y)].astype(jnp.float32)
+            + r2[k, block(z * 4 + r * 2 + y)].astype(jnp.float32)
+            + z2[k, block(r * 2 + y)].astype(jnp.float32)
             + x2[k, 0].astype(jnp.float32)
             + x2[k, 1].astype(jnp.float32)
             + x2[k, 3].astype(jnp.float32)
         ).astype(jnp.bfloat16)
 
-    for i in range(4):
-        for d in range(2):
-            first(i, d).wait_send()
-            relay(i, d).wait_send()
-    for copy in gather + tuple(stats) + spread:
+    for j in range(3):
+        for i in range(2):
+            along(i, j).wait_send()
+            over(i, j).wait_send()
+        for i in range(2, 5):
+            chunk(i, j).wait_send()
+    for copy in gather + tuple(stats) + near + far + (over_fs,):
         copy.wait_send()
     for k in range(4):
         merge_pair(k).wait_send()
         merge_far(k).wait_send()
+    for k in range(last):
         down_pair(k).wait_send()
+        down_fs(k).wait_send()
         for h in range(2):
             down_far(k, h).wait_send()
             down_via(k, h).wait_send()
@@ -476,13 +534,17 @@
     piece, local = direct_weight.shape
     wide = expand_weight.shape[1] // 2
     r = lax.axis_index("rep")
+    unit = wide // 2
+    f = lax.axis_index("fs")
     dv = jnp.concatenate([direct_weight.astype(bf), value_weight.astype(bf)], axis=1)
     dvscale = jnp.concatenate([direct_scale, value_scale])[None]
     sbias = jnp.repeat(jnp.transpose(spatial_bias), GDIM, axis=1)
     mg = (merge_weight * merge_scale).astype(bf)
     ex = lax.dynamic_slice_in_dim(expand_weight, r * wide, wide, 1).astype(bf)
-    exscale = lax.dynamic_slice_in_dim(expand_scale, r * wide, wide, 0)[None]
+    ex = jnp.stack([ex[:, :unit], ex[:, unit:]])
+    exscale = lax.dynamic_slice_in_dim(expand_scale, r * wide + f % 2 * unit, unit, 0)[None]
     rd = (lax.dynamic_slice_in_dim(reduce_weight, r * wide, wide, 0) * reduce_scale).astype(bf)
+    rd = jnp.transpose(rd.reshape(2, unit, 2, piece // 2), (0, 2, 1, 3))
     seq = 4 * rows
     vm = pltpu.VMEM
     dma = pltpu.SemaphoreType.DMA
@@ -499,8 +561,8 @@
         scratch_shapes=[
             vm((4, piece, 2 * local), bf),
             vm((4, local, piece), bf),
-            vm((4, piece, wide), bf),
-            vm((4, wide, piece), bf),
+            vm((4, piece, unit), bf),
+            vm((4, 2, unit, piece // 2), bf),
             vm((seq, width), bf),
             vm((seq, 2 * local), f32),
             vm((4, 4, 8, rows), f32),
@@ -510,20 +572,23 @@
             vm((4, rows, piece), bf),
             vm((4, rows, piece), bf),
             vm((rows, width), bf),
-            vm((2 * seq, width), bf),
-            vm((2 * seq, wide), f32),
-            vm((2 * seq, wide), bf),
-            vm((4, 2 * seq, piece), bf),
-            vm((4, seq, piece), bf),
-            vm((4, seq, piece), bf),
-            vm((4, 4, rows, piece), bf),
+            vm((4 * seq, width), bf),
+            vm((4 * seq, unit), f32),
+            vm((4 * seq, unit), bf),
+            vm((8, 4 * seq, piece // 2), bf),
+            vm((8, 2 * seq, piece // 2), bf),
+            vm((8, seq, piece // 2), bf),
+            vm((8, seq, piece // 2), bf),
+            vm((8, seq, piece // 2), bf),
+            vm((8, 4, rows, piece // 2), bf),
             dma((4,)),
-            dma((4, 2, 2)), dma((4, 2, 2)),
+            dma((5, 3)), dma((5, 3)),
+            dma((2, 3)), dma((2, 3)),
             dma((3,)), dma((3,)),
             dma((3,)), dma((3,)),
             dma((4, 2)), dma((4, 2)),
-            dma((8,)), dma((8,)),
-            dma((4, 7)), dma((4, 7)),
+            dma((17,)), dma((17,)),
+            dma((8, 8)), dma((8, 8)),
         ],
         compiler_params=pltpu.CompilerParams(
             collective_id=0, has_side_effects=True, vmem_limit_bytes=60 * 1024 * 1024

time: 226 us -> 217 us (0.960)
  Pallas kernels: 211 us -> 206 us
  other arithmetic: 7.72 us -> 3.59 us
    pallas_call x1, Pallas kernels: 211 us -> 206 us  [fused_body(): pl.pallas_call(fused_kernel, out_shape=jax.ShapeDtypeStruct((rows, width)...]
where the time goes in v2:
time: 217 us
  Pallas kernels  206 us (95%)
  local copies, waits for them, and re-layouts  7.47 us (3%)
  other arithmetic  3.59 us (2%)
    pallas_call x1, Pallas kernels, fused_body(): pl.pallas_call(fused_kernel, out_shape=jax.ShapeDtypeStruct((rows, width)...  206 us

profile of v2, /device:TPU:0, one launch (start us, length us, event | category | flops | bytes accessed | tf_op | source)
XLA Modules:
  0.0 216.8 jit_solution(10572792944633180279)
XLA Ops:
  0.0 0.0 copy-start.4
  0.0 1.4 dynamic_slice.10
  1.4 0.0 copy-start
  1.4 1.9 dynamic-slice_convert_fusion
  3.3 0.1 slice_bitcast_fusion.1
  3.3 1.1 pad_maximum_fusion.ex_ref
  4.4 0.0 copy-done.4
  4.4 0.0 copy-done
  4.4 0.0 copy-start.1
  4.4 0.0 copy-start.2
  4.4 0.3 multiply_convert_fusion
  4.7 0.0 copy-start.5
  4.7 0.0 copy-start.6
  4.7 0.0 copy-start.7
  4.8 0.0 copy-start.8
  4.8 0.3 reshape.9
  5.1 0.0 copy-start.3
  5.1 1.2 copy.22
  6.2 0.0 copy-done.1
  6.3 0.0 copy-done.2
  6.3 0.8 pad_maximum_fusion.1.dv_ref
  7.2 0.0 copy-done.5
  7.2 0.8 copy.20.sbias_ref
  7.9 0.0 copy-done.6
  7.9 0.0 copy-done.3
  7.9 0.7 multiply_convert_fusion.1.mg_ref
  8.7 0.0 copy-done.7
  8.7 0.0 copy-done.8
  8.7 0.6 pad_maximum_fusion.2
  9.3 205.6 %shard_map.163 = bf16[128,2048]{1,0:T(8,128)(2,1)} custom-call(bf16[128,2048]{1,0:T(8,128)(2,1)} %tok_ref.1, f32[1,2048]{1,0:T(1,128)} %bitcast.17, bf16[512,512]{1,0:T(8,128)(2,1)} %pad_maximum_fusion.1.dv_ref, f32[1,512]{1,0:T(1,128)} %bitcast.20, f32[1,256]{1,0:T(1,128)} %bitcast.22, f32[1,256]{1,0:T(1,128)} %bitcast.23, bf16[4,128,128]{2,1,0:T(8,128)(2,1)} %sw_ref.1, ...), custom_call_target="tpu_custom_call" | custom-call | tf_op jit(solution)/shard_map/pallas_call | solution.py:556
  214.9 1.9 copy.24
  (3 shorter events, 0.1 us)
Async XLA Ops:
  0.0 4.4 %copy-start.4 = (f32[512]{0:T(512)S(1)}, f32[512]{0:T(512)}, u32[]{:S(2)}) copy-start(f32[512]{0:T(512)} %param.33) | copy-start | bytes 6148
  1.4 3.0 %copy-start = (f32[2048,512]{1,0:T(8,128)S(1)}, f32[2048,512]{1,0:T(8,128)}, u32[]{:S(2)}) copy-start(f32[2048,512]{1,0:T(8,128)} %param.32) | copy-start | bytes 12582916
  4.4 1.8 copy-start.1
  4.4 1.9 copy-start.2
  4.7 2.4 %copy-start.5 = (f32[4,128]{1,0:T(4,128)S(1)}, f32[4,128]{1,0:T(4,128)}, u32[]{:S(2)}) copy-start(f32[4,128]{1,0:T(4,128)} %param.26) | copy-start | bytes 6148
  4.7 3.2 %copy-start.6 = (f32[512]{0:T(512)S(1)}, f32[512]{0:T(512)}, u32[]{:S(2)}) copy-start(f32[512]{0:T(512)} %param.28) | copy-start | bytes 6148
  4.7 3.9 %copy-start.7 = (f32[256]{0:T(256)S(1)}, f32[256]{0:T(256)}, u32[]{:S(2)}) copy-start(f32[256]{0:T(256)} %param.22) | copy-start | bytes 3076
  4.8 3.9 %copy-start.8 = (f32[256]{0:T(256)S(1)}, f32[256]{0:T(256)}, u32[]{:S(2)}) copy-start(f32[256]{0:T(256)} %param.20) | copy-start | bytes 3076
  5.1 2.9 %copy-start.3 = (f32[256,512]{1,0:T(8,128)S(1)}, f32[256,512]{1,0:T(8,128)}, u32[]{:S(2)}) copy-start(f32[256,512]{1,0:T(8,128)} %param.27) | copy-start | bytes 1572868

commit v3 on v2

--- a/solution.py
+++ b/solution.py
@@ -185,9 +185,8 @@
     for i in range(2):
         for j in range(3):
             along(i, j).start()
-    for i in range(2, 5):
-        for j in range(3):
-            chunk(i, j).start()
+    for j in range(3):
+        chunk(2, j).start()
     owns = [
         pltpu.make_async_copy(src, dst.at[f], own_sem.at[i])
         for i, (src, dst) in enumerate(
@@ -340,6 +339,9 @@
 
     near, far = spreading(0, z), spreading(1, 1 - z)
     over_fs.start()
+    for i in range(3, 5):
+        for j in range(3):
+            chunk(i, j).start()
     for k in range(3):
         near[k].start()
     over_fs.wait_recv()

time: 217 us -> 190 us (0.88)
  Pallas kernels: 206 us -> 179 us
    pallas_call x1, Pallas kernels: 206 us -> 179 us  [fused_body(): pl.pallas_call(fused_kernel, out_shape=jax.ShapeDtypeStruct((rows, width)...]
where the time goes in v3:
time: 190 us
  Pallas kernels  179 us (94%)
  local copies, waits for them, and re-layouts  7.47 us (4%)
  other arithmetic  3.59 us (2%)
    pallas_call x1, Pallas kernels, fused_body(): pl.pallas_call(fused_kernel, out_shape=jax.ShapeDtypeStruct((rows, width)...  179 us

profile of v3, /device:TPU:0, one launch (start us, length us, event | category | flops | bytes accessed | tf_op | source)
XLA Modules:
  0.0 189.7 jit_solution(1179295149455482999)
XLA Ops:
  0.0 0.0 copy-start.4
  0.0 1.4 dynamic_slice.10
  1.4 0.0 copy-start
  1.4 1.9 dynamic-slice_convert_fusion
  3.3 0.1 slice_bitcast_fusion.1
  3.3 1.1 pad_maximum_fusion.ex_ref
  4.4 0.0 copy-done.4
  4.4 0.0 copy-done
  4.4 0.0 copy-start.1
  4.4 0.0 copy-start.2
  4.4 0.3 multiply_convert_fusion
  4.7 0.0 copy-start.5
  4.7 0.0 copy-start.6
  4.7 0.0 copy-start.7
  4.8 0.0 copy-start.8
  4.8 0.3 reshape.9
  5.1 0.0 copy-start.3
  5.1 1.2 copy.22
  6.2 0.0 copy-done.1
  6.3 0.0 copy-done.2
  6.3 0.8 pad_maximum_fusion.1.dv_ref
  7.2 0.0 copy-done.5
  7.2 0.8 copy.20.sbias_ref
  7.9 0.0 copy-done.6
  7.9 0.0 copy-done.3
  7.9 0.7 multiply_convert_fusion.1.mg_ref
  8.7 0.0 copy-done.7
  8.7 0.0 copy-done.8
  8.7 0.6 pad_maximum_fusion.2
  9.3 178.5 %shard_map.163 = bf16[128,2048]{1,0:T(8,128)(2,1)} custom-call(bf16[128,2048]{1,0:T(8,128)(2,1)} %tok_ref.1, f32[1,2048]{1,0:T(1,128)} %bitcast.17, bf16[512,512]{1,0:T(8,128)(2,1)} %pad_maximum_fusion.1.dv_ref, f32[1,512]{1,0:T(1,128)} %bitcast.20, f32[1,256]{1,0:T(1,128)} %bitcast.22, f32[1,256]{1,0:T(1,128)} %bitcast.23, bf16[4,128,128]{2,1,0:T(8,128)(2,1)} %sw_ref.1, ...), custom_call_target="tpu_custom_call" | custom-call | tf_op jit(solution)/shard_map/pallas_call | solution.py:558
  187.8 1.9 copy.24
  (3 shorter events, 0.1 us)
Async XLA Ops:
  0.0 4.4 %copy-start.4 = (f32[512]{0:T(512)S(1)}, f32[512]{0:T(512)}, u32[]{:S(2)}) copy-start(f32[512]{0:T(512)} %param.33) | copy-start | bytes 6148
  1.4 3.0 %copy-start = (f32[2048,512]{1,0:T(8,128)S(1)}, f32[2048,512]{1,0:T(8,128)}, u32[]{:S(2)}) copy-start(f32[2048,512]{1,0:T(8,128)} %param.32) | copy-start | bytes 12582916
  4.4 1.8 copy-start.1
  4.4 1.9 copy-start.2
  4.7 2.4 %copy-start.5 = (f32[4,128]{1,0:T(4,128)S(1)}, f32[4,128]{1,0:T(4,128)}, u32[]{:S(2)}) copy-start(f32[4,128]{1,0:T(4,128)} %param.26) | copy-start | bytes 6148
  4.7 3.2 %copy-start.6 = (f32[512]{0:T(512)S(1)}, f32[512]{0:T(512)}, u32[]{:S(2)}) copy-start(f32[512]{0:T(512)} %param.28) | copy-start | bytes 6148
  4.7 3.9 %copy-start.7 = (f32[256]{0:T(256)S(1)}, f32[256]{0:T(256)}, u32[]{:S(2)}) copy-start(f32[256]{0:T(256)} %param.22) | copy-start | bytes 3076
  4.8 3.9 %copy-start.8 = (f32[256]{0:T(256)S(1)}, f32[256]{0:T(256)}, u32[]{:S(2)}) copy-start(f32[256]{0:T(256)} %param.20) | copy-start | bytes 3076
  5.1 2.9 %copy-start.3 = (f32[256,512]{1,0:T(8,128)S(1)}, f32[256,512]{1,0:T(8,128)}, u32[]{:S(2)}) copy-start(f32[256,512]{1,0:T(8,128)} %param.27) | copy-start | bytes 1572868
